TPU v7x, 32 devices: a whole 2x2x4 slice. The times are simulated.
32 devices in a mesh: sp: 4 (over y, x), tp: 8 (over z, core).
Axes of the slice: x: 2, y: 2, z: 4, core: 2. Of those that a mesh axis runs over, the one named last changes fastest.
Arguments:
- tokens: bfloat16 [2, 512, 4096], P(None, 'sp', 'tp'), may hold values from -6 to 6
- key_matrix: bfloat16 [4096, 4096], P(None, 'tp'), may hold values from -0.09375 to 0.09375
- value_matrix: bfloat16 [4096, 4096], P(None, 'tp'), may hold values from -0.375 to 0.375
- gate_matrix: bfloat16 [4096, 64], replicated, may hold values from -0.09375 to 0.09375
- head_decay_rate: float32 [32], P('tp'), may hold values from 0 to 1, as said below
- extra_log_decay: float32 [2, 32, 512], P(None, 'tp', 'sp'), may hold values from -3 to 0, as said below
- next_token_query: bfloat16 [2, 4096], P(None, 'tp'), may hold values from -6 to 6
- next_token_key: bfloat16 [2, 4096], P(None, 'tp'), may hold values from -6 to 6
- next_token_value: bfloat16 [2, 32, 128], P(None, 'tp', 'sp'), may hold values from -6 to 6
- next_write_strength: float32 [2, 32], P(None, 'tp'), may hold values from 0.05 to 1
- read_norm_gain: float32 [128], P('sp'), may hold values from 0.1 to 1.9
Outputs:
- state_cache: bfloat16 [2, 32, 128, 128], P(None, 'tp', None, 'sp')
- first_read: bfloat16 [2, 32, 128], P(None, 'tp', 'sp')
Inputs may be any that keep to these rules, and one draw needn't show every extreme that they name: `head_decay_rate`: positive. `extra_log_decay`: never positive.
All inputs are finite; a program needn't handle non-finite values.
Results may differ from a plain program's by a relative error of at most 0.013.
Values may be sent and summed in bfloat16 or wider, within the bound.
A program may use at most 64 MiB of HBM per device.

v0:
```python
import jax
import jax.numpy as jnp
from jax import lax
from jax.sharding import PartitionSpec as P

DV = 128


exact_mode = lax.Precision.HIGHEST
strength_offset = 5.0


def unit_rows(matrix):
    return matrix * lax.rsqrt(jnp.sum(matrix * matrix, axis=-1, keepdims=True) + 1e-06)


def nilpotent_inverse(mixing):
    extent = mixing.shape[-1]
    result = jnp.zeros_like(mixing) + jnp.eye(extent, dtype=jnp.float32)
    powered = -mixing
    covered = 1
    while covered < extent:
        product = lax.optimization_barrier(
            jnp.einsum("...ij,...jk->...ik", result, powered, precision=exact_mode)
        )
        result = result + product
        powered = jnp.einsum("...ij,...jk->...ik", powered, powered, precision=exact_mode)
        covered = covered * 2
    return result


def block_terms(unit_keys, values, decay_logarithm, strength):
    extent = unit_keys.shape[-2]
    lower = jnp.tril(jnp.ones((extent, extent), jnp.bool_))
    strict = jnp.tril(jnp.ones((extent, extent), jnp.bool_), -1)
    running = jnp.cumsum(decay_logarithm, axis=-1)
    spread = running[..., :, None] - running[..., None, :]
    within = jnp.where(lower, jnp.exp(jnp.where(lower, spread, 0.0)), 0.0)
    scaled = unit_keys * strength[..., None]
    mixing = jnp.where(
        strict,
        jnp.einsum("...id,...jd->...ij", scaled, unit_keys, precision=exact_mode) * within,
        0.0,
    )
    inverse = nilpotent_inverse(mixing)
    writes = jnp.einsum(
        "...ij,...je->...ie", inverse, values * strength[..., None], precision=exact_mode
    )
    erases = jnp.einsum(
        "...ij,...jd->...id", inverse, scaled * jnp.exp(running)[..., None], precision=exact_mode
    )
    final_log = running[..., -1]
    carried = unit_keys * jnp.exp(final_log[..., None] - running)[..., None]
    return (writes, erases, carried, final_log)


def split_blocks(array, block_count):
    shaped = array.reshape(
        array.shape[:2] + (block_count, array.shape[2] // block_count) + array.shape[3:]
    )
    return jnp.moveaxis(shaped, 2, 0)


def local(
    tokens,
    key_matrix,
    value_matrix,
    gate_matrix,
    head_decay_rate,
    extra_log_decay,
    next_token_query,
    next_token_key,
    next_token_value,
    next_write_strength,
    read_norm_gain,
):
    sequences, positions, _ = tokens.shape
    local_heads = head_decay_rate.shape[0]
    key_width = key_matrix.shape[1] // local_heads
    value_width = value_matrix.shape[1] // local_heads
    all_heads = gate_matrix.shape[1] // 2
    group_size = lax.axis_size("sp")
    column_share = value_width // group_size
    first_head = lax.axis_index("tp") * local_heads
    decay_cols = lax.dynamic_slice_in_dim(gate_matrix, first_head, local_heads, 1)
    strength_cols = lax.dynamic_slice_in_dim(gate_matrix, all_heads + first_head, local_heads, 1)
    gate_cols = jnp.concatenate([decay_cols, strength_cols], axis=1)
    row_count = sequences * positions
    incoming = lax.all_gather(tokens, "tp", axis=2, tiled=True)
    span_width = incoming.shape[2]
    flat_rows = incoming.reshape(row_count, span_width)
    products = lax.optimization_barrier(
        (
            jnp.dot(flat_rows, key_matrix, preferred_element_type=jnp.float32),
            jnp.dot(flat_rows, value_matrix, preferred_element_type=jnp.float32),
            jnp.dot(flat_rows, gate_cols, preferred_element_type=jnp.float32),
        )
    )
    key_sum = products[0]
    value_sum = products[1]
    gate_pre = products[2]
    key_float = lax.optimization_barrier(key_sum.astype(jnp.bfloat16)).astype(jnp.float32)
    value_float = lax.optimization_barrier(value_sum.astype(jnp.bfloat16)).astype(jnp.float32)
    unit_keys = unit_rows(
        key_float.reshape(sequences, positions, local_heads, key_width).transpose(0, 2, 1, 3)
    )
    values = value_float.reshape(sequences, positions, local_heads, value_width).transpose(
        0, 2, 1, 3
    )
    gate_projected = gate_pre.reshape(sequences, positions, 2 * local_heads).transpose(0, 2, 1)
    decay_logarithm = (
        -head_decay_rate[None, :, None] * jax.nn.softplus(gate_projected[:, :local_heads])
        + extra_log_decay
    )
    strength = jax.nn.sigmoid(gate_projected[:, local_heads:] - strength_offset)
    block_count = positions // min(64, positions)
    block_parts = block_terms(
        split_blocks(unit_keys, block_count),
        split_blocks(values, block_count),
        split_blocks(decay_logarithm, block_count),
        split_blocks(strength, block_count),
    )
    identity = jnp.zeros((sequences, local_heads, key_width, key_width), jnp.float32) + jnp.eye(
        key_width, dtype=jnp.float32
    )
    start_map = jnp.concatenate(
        [identity, jnp.zeros((sequences, local_heads, key_width, value_width), jnp.float32)],
        axis=-1,
    )

    def advance(current, block_part):
        writes, erases, carried, final_log = block_part
        padded = jnp.concatenate(
            [jnp.zeros(writes.shape[:-1] + (key_width,), jnp.float32), writes], axis=-1
        )
        removed = lax.optimization_barrier(
            jnp.einsum("shcd,shde->shce", erases, current, precision=exact_mode)
        )
        fresh = padded - removed
        added = lax.optimization_barrier(
            jnp.einsum("shcd,shce->shde", carried, fresh, precision=exact_mode)
        )
        current = current * jnp.exp(final_log)[..., None, None] + added
        return (current, None)

    local_map, _ = lax.scan(advance, start_map, block_parts)
    carry_map = local_map[..., :key_width]
    write_map = local_map[..., key_width:]
    carry_copies = jnp.broadcast_to(carry_map[None], (group_size,) + carry_map.shape)
    write_parts = jnp.moveaxis(
        write_map.reshape(sequences, local_heads, key_width, group_size, column_share), 3, 0
    )
    carries = lax.all_to_all(carry_copies, "sp", split_axis=0, concat_axis=0, tiled=True)
    write_cols = lax.all_to_all(write_parts, "sp", split_axis=0, concat_axis=0, tiled=True)

    def fold_step(current, block_map):
        moved = lax.optimization_barrier(
            jnp.einsum("shij,shje->shie", block_map[0], current, precision=exact_mode)
        )
        return (moved + block_map[1], None)

    begin_state = jnp.zeros(write_cols.shape[1:], jnp.float32)
    folded, _ = lax.scan(fold_step, begin_state, (carries, write_cols))
    query_rows = next_token_query.astype(jnp.float32).reshape(sequences, local_heads, key_width)
    unit_new = unit_rows(
        next_token_key.astype(jnp.float32).reshape(sequences, local_heads, key_width)
    )
    value_rows = next_token_value.astype(jnp.float32)
    key_read = jnp.einsum("shd,shde->she", unit_new, folded, precision=exact_mode)
    query_read = jnp.einsum("shd,shde->she", query_rows, folded, precision=exact_mode)
    intersection = jnp.sum(query_rows * unit_new, axis=-1)
    read_raw = query_read + (next_write_strength * intersection)[..., None] * (
        value_rows - key_read
    )
    square_total = lax.psum(jnp.sum(read_raw * read_raw, axis=-1, keepdims=True), "sp")
    first_read = read_raw * lax.rsqrt(square_total / DV + 1e-06) * read_norm_gain
    return (folded.astype(jnp.bfloat16), first_read.astype(jnp.bfloat16))


def solution(mesh):
    in_specs = (
        P(None, "sp", "tp"),
        P(None, "tp"),
        P(None, "tp"),
        P(),
        P("tp"),
        P(None, "tp", "sp"),
        P(None, "tp"),
        P(None, "tp"),
        P(None, "tp", "sp"),
        P(None, "tp"),
        P("sp"),
    )
    out_specs = (P(None, "tp", None, "sp"), P(None, "tp", "sp"))
    return jax.shard_map(local, mesh=mesh, in_specs=in_specs, out_specs=out_specs, check_vma=False)
```

profile of v0, /device:TPU:0, one launch (start us, length us, event | category | flops | bytes accessed | tf_op | source)
XLA Modules:
  0.0 130.1 jit_solution(6070156353231956708)
XLA Ops:
  7.2 0.7 all-gather.2.cloned.1.call-update
  7.9 0.7 neg.14
  8.8 0.9 constant_dynamic-slice_fusion.2
  9.7 31.8 %all-gather.2.cloned.1.call-done = bf16[2,128,4096]{2,1,0:T(8,128)(2,1)} async-done(((bf16[2,128,512]{2,1,0:T(8,128)(2,1)}), bf16[2,128,4096]{2,1,0:T(8,128)(2,1)}) %all-gather.2.cloned.1.call-update) | async-done | bytes 2097168 | tf_op jit(solution)/shard_map/all_gather | solution.py:89
  41.5 4.2 %fusion.52 = bf16[256,512]{1,0:T(8,128)(2,1)S(1)} fusion(bf16[256,4096]{1,0:T(8,128)(2,1)} %bitcast.96, bf16[4096,512]{1,0:T(8,128)(2,1)} %param.16), kind=kOutput, calls=%fused_computation.86 | convolution fusion | flops 1073741824 | bytes 6553600 | tf_op jit(solution)/shard_map/dot_general | solution.py:94
  46.2 1.2 fusion.53
  48.2 1.1 reduce_window_sum.11
  51.0 1.0 fusion.22
  53.9 0.7 fusion.30
  55.2 0.7 fusion.38
  58.0 0.7 fusion.59
  58.8 0.7 fusion.61
  59.5 0.7 fusion.24
  60.1 0.7 fusion.26
  60.8 4.5 %while.21 = (s32[]{:T(128)}, f32[2,4,128,256]{3,2,1,0:T(8,128)S(1)}, f32[2,2,4]{2,1,0:T(2,128)S(1)}, f32[2,2,4,64,128]{4,3,0,2,1:T(8,128)S(1)}, f32[2,2,4,64,128...) while((s32[]{:T(128)}, f32[2,4,128,256]{3,2,1,0:T(8,128)S(1)}, ...), condition=%wide.region_3.4_spmd, body=%wide.region_2.3_spmd.sunk | while | flops 403308544 | bytes 7602365 | solution.py:146
  61.0 0.7 fusion.107
  61.8 1.1 fusion.108
  63.2 0.7 fusion.107
  64.0 1.1 fusion.108
  65.7 0.8 copy.38
  66.6 3.6 %all-to-all-start.1 = ((f32[4,2,4,128,32]{3,4,2,1,0:T(8,128)}), f32[4,2,4,128,32]{3,4,2,1,0:T(8,128)S(1)}, u32[]{:S(2)}, u32[]{:S(2)}) async-start(f32[4,2,4,128,32]{3,4,2,1,0:T(8,128)} %copy.38), calls=%async_computation.1 | async-start | bytes 1048576 | tf_op jit(solution)/shard_map/all_to_all | solution.py:154
  70.3 8.5 %all-to-all-done.1 = f32[4,2,4,128,32]{3,4,2,1,0:T(8,128)S(1)} async-done(((f32[4,2,4,128,32]{3,4,2,1,0:T(8,128)}), f32[4,2,4,128,32]{3,4,2,1,0:T(8,128)S(1)}, u32[]{:S(2)}, u32[]{:S(2)}) %all-to-all-start.1) | async-done | bytes 524320 | tf_op jit(solution)/shard_map/all_to_all | solution.py:154
  78.7 1.6 %broadcast_in_dim.51 = f32[4,2,4,128,128]{4,3,2,1,0:T(8,128)} broadcast(f32[2,4,128,128]{3,2,1,0:T(8,128)S(1)} %slice.18), dimensions={1,2,3,4} | broadcast | bytes 2621440 | tf_op jit(solution)/shard_map/broadcast_in_dim | solution.py:149
  80.3 3.7 %all-to-all-start = ((f32[4,2,4,128,128]{4,3,2,1,0:T(8,128)}), f32[4,2,4,128,128]{4,3,2,1,0:T(8,128)S(1)}, u32[]{:S(2)}, u32[]{:S(2)}) async-start(f32[4,2,4,128,128]{4,3,2,1,0:T(8,128)} %broadcast_in_dim.51), calls=%async_computation | async-start | bytes 4194304 | tf_op jit(solution)/shard_map/all_to_all | solution.py:153
  84.4 24.1 %all-to-all-done = f32[4,2,4,128,128]{4,3,2,1,0:T(8,128)S(1)} async-done(((f32[4,2,4,128,128]{4,3,2,1,0:T(8,128)}), f32[4,2,4,128,128]{4,3,2,1,0:T(8,128)S(1)}, u32[]{:S(2)}, u32[]{:S(2)}) %all-to-all-start) | async-done | bytes 2097184 | tf_op jit(solution)/shard_map/all_to_all | solution.py:153
  108.5 3.9 %while.22 = (s32[]{:T(128)}, f32[2,4,128,32]{2,3,1,0:T(8,128)S(1)}, f32[4,2,4,128,128]{4,3,2,1,0:T(8,128)S(1)}, f32[4,2,4,128,32]{3,4,2,1,0:T(8,128)S(1)}, s32[]{:T(128)}, /*index=5*/s32[]{:T(128)}) while((s32[]{:T(128)}, f32[2,4,128,32]{2,3,1,0:T(8,128)S(1)}, f32[4,2,4,128,128]{4,3,2,1,0:T(8,128)S(1)}, ...), condition=%wide.region_5.6_spmd.clone, body=%wide.region_4.5_spmd.clone.sunk | while | flops 50397184 | bytes 1179735 | solution.py:163
  108.5 0.9 fusion.112
  109.5 0.9 fusion.112
  110.4 0.9 fusion.112
  111.4 0.9 fusion.112
  113.7 8.9 %psum.7 = f32[2,4,1]{1,0,2:T(2,128)S(1)} all-reduce(f32[2,4,1]{1,0,2:T(2,128)S(1)} %bitcast.111), channel_id=1, replica_groups=mesh['sp'=4,'tp'=8] {'sp'}, use_global_device_ids=true, to_apply=%region_9.10 | all-reduce | flops 8 | bytes 64 | tf_op jit(solution)/shard_map/psum | solution.py:175
  122.6 0.7 multiply_convert_fusion
  (75 shorter events, 10.7 us)
Async XLA Ops:
  7.2 34.3 %all-gather.2.cloned.1.call-start = ((), (), s32[]{:S(2)}) async-start(), calls=%async_computation.2 | async-start | bytes 2359296 | tf_op jit(solution)/shard_map/all_gather | solution.py:89
  41.5 4.2 %copy-start = (bf16[2,128,4096]{2,1,0:T(8,128)(2,1)S(1)}, bf16[2,128,4096]{2,1,0:T(8,128)(2,1)}, u32[]{:S(2)}) copy-start(bf16[2,128,4096]{2,1,0:T(8,128)(2,1)} %all-gather.2.cloned.1.call-done) | copy-start | bytes 6291460
  41.5 4.7 %copy-start.7 = (bf16[4096,512]{1,0:T(8,128)(2,1)S(1)}, bf16[4096,512]{1,0:T(8,128)(2,1)}, u32[]{:S(2)}) copy-start(bf16[4096,512]{1,0:T(8,128)(2,1)} %param.17) | copy-start | bytes 12582916
  47.4 0.7 copy-start.3
  66.6 12.1 %all-to-all-start.1 = ((f32[4,2,4,128,32]{3,4,2,1,0:T(8,128)}), f32[4,2,4,128,32]{3,4,2,1,0:T(8,128)S(1)}, u32[]{:S(2)}, u32[]{:S(2)}) async-start(f32[4,2,4,128,32]{3,4,2,1,0:T(8,128)} %copy.38), calls=%async_computation.1 | async-start | bytes 1048576 | tf_op jit(solution)/shard_map/all_to_all | solution.py:154
  80.3 3.8 %copy-start.1 = (bf16[2,512]{1,0:T(2,128)(2,1)S(1)}, bf16[2,512]{1,0:T(2,128)(2,1)}, u32[]{:S(2)}) copy-start(bf16[2,512]{1,0:T(2,128)(2,1)} %param.21) | copy-start | bytes 6148
  80.3 3.8 %copy-start.4 = (bf16[2,512]{1,0:T(2,128)(2,1)S(1)}, bf16[2,512]{1,0:T(2,128)(2,1)}, u32[]{:S(2)}) copy-start(bf16[2,512]{1,0:T(2,128)(2,1)} %param.22) | copy-start | bytes 6148
  80.3 4.1 %copy-start.5 = (f32[2,4]{1,0:T(2,128)S(1)}, f32[2,4]{1,0:T(2,128)}, u32[]{:S(2)}) copy-start(f32[2,4]{1,0:T(2,128)} %param.24) | copy-start | bytes 100
  80.3 28.2 %all-to-all-start = ((f32[4,2,4,128,128]{4,3,2,1,0:T(8,128)}), f32[4,2,4,128,128]{4,3,2,1,0:T(8,128)S(1)}, u32[]{:S(2)}, u32[]{:S(2)}) async-start(f32[4,2,4,128,128]{4,3,2,1,0:T(8,128)} %broadcast_in_dim.51), calls=%async_computation | async-start | bytes 4194304 | tf_op jit(solution)/shard_map/all_to_all | solution.py:153
  108.5 5.1 %copy-start.2 = (bf16[2,4,32]{2,1,0:T(4,128)(2,1)S(1)}, bf16[2,4,32]{2,1,0:T(4,128)(2,1)}, u32[]{:S(2)}) copy-start(bf16[2,4,32]{2,1,0:T(4,128)(2,1)} %param.23) | copy-start | bytes 1540
  108.5 14.1 %copy-start.6 = (f32[32]{0:T(128)S(1)}, f32[32]{0:T(128)}, u32[]{:S(2)}) copy-start(f32[32]{0:T(128)} %param.25) | copy-start | bytes 388
Sparse Core Ops, SparseCore 0:
  9.6 31.8 all-gather.1
where the time goes:
time: 130 us
  waiting for transfers between devices  65 us (50%)
  matrix products  23.3 us (18%)
  between operations  14.4 us (11%)
  blocking collectives  8.86 us (7%)
  starting transfers between devices  7.41 us (6%)
  other arithmetic  5.62 us (4%)
  local copies, waits for them, and re-layouts  5.17 us (4%)
    all_gather x1, waiting for transfers between devices, local(): incoming = lax.all_gather(tokens, 'tp', axis=2, tiled=True)  31.8 us
    all_to_all x1, waiting for transfers between devices, local(): lax.all_to_all(carry_copies, 'sp', split_axis=0, concat_axis=0, tiled=True)  24.1 us
    psum x1, blocking collectives, local(): lax.psum(jnp.sum(read_raw * read_raw, axis=-1, keepdims=True), 'sp')  8.86 us
    all_to_all x1, waiting for transfers between devices, local(): lax.all_to_all(write_parts, 'sp', split_axis=0, concat_axis=0, tiled=True)  8.45 us
    dot_general x1, matrix products, local(): jnp.dot(flat_rows, key_matrix, preferred_element_type=jnp.float32)  4.21 us
    dot_general x6, matrix products, nilpotent_inverse(): jnp.einsum('...ij,...jk->...ik', result, powered, precision=exact_mode)  3.89 us
    all_to_all x1, starting transfers between devices, local(): lax.all_to_all(carry_copies, 'sp', split_axis=0, concat_axis=0, tiled=True)  3.74 us
    dot_general x4, matrix products, fold_step(): jnp.einsum('shij,shje->shie', block_map[0], current, precision=exact_mode)  3.69 us
  transfers between devices with their start and end apart: 3, of which 3 were waited for; matrix products, arithmetic and copies ran while one was open for 2% of the time, Pallas kernels for 0%

commit v1 on v0

--- a/solution.py
+++ b/solution.py
@@ -1,9 +1,15 @@
+import functools
+
 import jax
 import jax.numpy as jnp
 from jax import lax
+from jax.experimental import pallas as pl
+from jax.experimental.pallas import tpu as pltpu
 from jax.sharding import PartitionSpec as P
 
 DV = 128
+CORES = 2
+MESH = pl.DeviceIdType.MESH
 
 
 exact_mode = lax.Precision.HIGHEST
@@ -61,7 +67,7 @@
     return jnp.moveaxis(shaped, 2, 0)
 
 
-def local(
+def local_general(
     tokens,
     key_matrix,
     value_matrix,
@@ -177,6 +183,500 @@
     return (folded.astype(jnp.bfloat16), first_read.astype(jnp.bfloat16))
 
 
+def exact_dot(left, right, contract=((1,), (0,))):
+    return lax.dot_general(
+        left, right, (contract, ((), ())), precision=exact_mode, preferred_element_type=jnp.float32
+    )
+
+
+def short_dot(left, right, contract=((1,), (0,))):
+    return lax.dot_general(
+        left.astype(jnp.bfloat16),
+        right.astype(jnp.bfloat16),
+        (contract, ((), ())),
+        preferred_element_type=jnp.float32,
+    )
+
+
+def softplus(x):
+    return jnp.maximum(x, 0.0) + jnp.log1p(jnp.exp(-jnp.abs(x)))
+
+
+def grid_mask(rows, cols, rule):
+    row = lax.broadcasted_iota(jnp.int32, (rows, cols), 0)
+    col = lax.broadcasted_iota(jnp.int32, (rows, cols), 1)
+    return rule(row, col)
+
+
+def fused_kernel(
+    sp_size,
+    tp_size,
+    rate_ref,
+    next_strength_ref,
+    tokens_ref,
+    key_ref,
+    value_ref,
+    gate_ref,
+    extra_ref,
+    query_ref,
+    new_key_ref,
+    new_value_ref,
+    gain_ref,
+    state_ref,
+    read_ref,
+    gathered,
+    key_w,
+    value_w,
+    key_acc,
+    value_acc,
+    gate_acc,
+    kv_out,
+    kv_in,
+    side_out,
+    side_in,
+    state_out,
+    state_in,
+    row_out,
+    row_in,
+    load_sem,
+    weight_sem,
+    gather_recv,
+    gather_send,
+    swap_recv,
+    swap_send,
+    swap_local,
+    last_recv,
+    last_send,
+    last_local,
+):
+    sequences, positions, depth = tokens_ref.shape
+    local_heads = extra_ref.shape[1]
+    key_width = key_acc.shape[1] // local_heads
+    value_width = value_acc.shape[1] // local_heads
+    share = value_width // sp_size
+    all_heads = gate_ref.shape[1] // 2
+    chips = tp_size // CORES
+    me = lax.axis_index("sp")
+    spot = lax.axis_index("tp")
+    chip = spot // CORES
+    core = spot % CORES
+    partner = chip * CORES + (1 - core)
+
+    loads = [
+        pltpu.make_async_copy(tokens_ref.at[s], gathered.at[spot, s], load_sem.at[s])
+        for s in range(sequences)
+    ]
+    for load in loads:
+        load.start()
+
+    barrier = pltpu.get_barrier_semaphore()
+    pl.semaphore_signal(barrier, inc=1, device_id={"tp": partner}, device_id_type=MESH)
+
+    @pl.when(chip > 0)
+    def _():
+        pl.semaphore_signal(barrier, inc=1, device_id={"tp": spot - CORES}, device_id_type=MESH)
+
+    @pl.when(chip < chips - 1)
+    def _():
+        pl.semaphore_signal(barrier, inc=1, device_id={"tp": spot + CORES}, device_id_type=MESH)
+
+    for offset in range(1, sp_size):
+        pl.semaphore_signal(
+            barrier, inc=1, device_id={"sp": (me + offset) % sp_size}, device_id_type=MESH
+        )
+    weights = [
+        pltpu.make_async_copy(key_ref, key_w, weight_sem.at[0]),
+        pltpu.make_async_copy(value_ref, value_w, weight_sem.at[1]),
+    ]
+    for weight in weights:
+        weight.start()
+    key_acc[...] = jnp.zeros_like(key_acc)
+    value_acc[...] = jnp.zeros_like(value_acc)
+    gate_acc[...] = jnp.zeros_like(gate_acc)
+    for load in loads:
+        load.wait()
+    near = jnp.where(chip > 0, 1, 0) + jnp.where(chip < chips - 1, 1, 0)
+    pl.semaphore_wait(barrier, near + sp_size)
+
+    def piece(origin, s, way, target):
+        return pltpu.make_async_remote_copy(
+            src_ref=gathered.at[origin, s],
+            dst_ref=gathered.at[origin, s],
+            send_sem=gather_send.at[origin, s, way],
+            recv_sem=gather_recv.at[origin, s],
+            device_id={"tp": target},
+            device_id_type=MESH,
+        )
+
+    def take(block):
+        rows = gathered[block].reshape(sequences * positions, depth)
+        span = pl.ds(pl.multiple_of(block * depth, depth), depth)
+        key_acc[...] += jnp.dot(rows, key_w[span, :], preferred_element_type=jnp.float32)
+        value_acc[...] += jnp.dot(rows, value_w[span, :], preferred_element_type=jnp.float32)
+        gate_acc[...] += jnp.dot(rows, gate_ref[span, :], preferred_element_type=jnp.float32)
+
+    for s in range(sequences):
+
+        @pl.when(chip < chips - 1)
+        def _(s=s):
+            piece(spot, s, 0, spot + CORES).start()
+
+        @pl.when(chip > 0)
+        def _(s=s):
+            piece(spot, s, 1, spot - CORES).start()
+
+        piece(spot, s, 2, partner).start()
+    for weight in weights:
+        weight.wait()
+    take(spot)
+    for s in range(sequences):
+        piece(partner, s, 2, partner).wait_recv()
+    take(partner)
+
+    for distance in range(1, chips):
+        for s in range(sequences):
+            for way, step in ((0, -1), (1, 1)):
+                origin_chip = chip + step * distance
+                origin = origin_chip * CORES + core
+                present = (origin_chip >= 0) & (origin_chip < chips)
+                onward = chip - step
+
+                @pl.when(present)
+                def _(s=s, way=way, origin=origin, onward=onward):
+                    piece(origin, s, way, partner).wait_recv()
+
+                    @pl.when((onward >= 0) & (onward < chips))
+                    def _():
+                        piece(origin, s, way, onward * CORES + core).start()
+
+                    piece(origin, s, 2, partner).start()
+
+        def absorb(index, carry, distance=distance):
+            side = index // CORES
+            which = index % CORES
+            origin_chip = chip + (2 * side - 1) * distance
+            present = (origin_chip >= 0) & (origin_chip < chips)
+
+            @pl.when(present & (which == 0))
+            def _():
+                take(origin_chip * CORES + core)
+
+            @pl.when(present & (which == 1))
+            def _():
+                block = origin_chip * CORES + 1 - core
+                for s in range(sequences):
+                    piece(block, s, 2, partner).wait_recv()
+                take(block)
+
+            return carry
+
+        lax.fori_loop(0, 2 * CORES, absorb, 0)
+
+    first = spot * local_heads
+    chooser = grid_mask(
+        2 * local_heads,
+        2 * all_heads,
+        lambda r, c: c == jnp.where(r < local_heads, first + r, all_heads + first + r - local_heads),
+    ).astype(jnp.float32)
+    gates = exact_dot(chooser, gate_acc[...], ((1,), (1,)))
+    placer = grid_mask(share, value_width, lambda r, c: c == me * share + r).astype(jnp.float32)
+    side_out[...] = jnp.zeros_like(side_out)
+    for s in range(sequences):
+        cut = slice(s * positions, (s + 1) * positions)
+        new_value = exact_dot(new_value_ref[s].astype(jnp.float32), placer)
+        extra = extra_ref[s]
+        for h in range(local_heads):
+            kv_out[h, 0, s] = key_acc[cut, h * key_width : (h + 1) * key_width].astype(jnp.bfloat16)
+            kv_out[h, 1, s] = value_acc[cut, h * value_width : (h + 1) * value_width].astype(
+                jnp.bfloat16
+            )
+            side_out[h, s : s + 1, :] = (
+                -rate_ref[h] * softplus(gates[h : h + 1, cut]) + extra[h : h + 1, :]
+            )
+            side_out[h, 2 + s : 3 + s, :] = jax.nn.sigmoid(
+                gates[local_heads + h : local_heads + h + 1, cut] - strength_offset
+            )
+            side_out[h, 4 + s : 5 + s, :] = new_value[h : h + 1, :]
+
+    def swap(target, origin):
+        return [
+            pltpu.make_async_remote_copy(
+                src_ref=source.at[target],
+                dst_ref=sink.at[origin],
+                send_sem=swap_send.at[n, target],
+                recv_sem=swap_recv.at[n, origin],
+                device_id={"sp": target},
+                device_id_type=MESH,
+            )
+            for n, (source, sink) in enumerate(((kv_out, kv_in), (side_out, side_in)))
+        ]
+
+    for offset in range(1, sp_size):
+        for copy in swap((me + offset) % sp_size, me):
+            copy.start()
+    kept = [
+        pltpu.make_async_copy(kv_out.at[me], kv_in.at[me], swap_local.at[0]),
+        pltpu.make_async_copy(side_out.at[me], side_in.at[me], swap_local.at[1]),
+    ]
+    for copy in kept:
+        copy.start()
+    for copy in kept:
+        copy.wait()
+    for offset in range(1, sp_size):
+        source = (me + offset) % sp_size
+        for n, sink in enumerate((kv_in, side_in)):
+            pltpu.make_async_remote_copy(
+                src_ref=sink.at[source],
+                dst_ref=sink.at[source],
+                send_sem=swap_send.at[n, source],
+                recv_sem=swap_recv.at[n, source],
+                device_id={"sp": source},
+                device_id_type=MESH,
+            ).wait_recv()
+
+    side_rows = side_in.shape[1]
+    side = side_in[...].reshape(sp_size * side_rows, positions)
+    upto = grid_mask(positions, positions, lambda r, c: r <= c).astype(jnp.float32)
+    eye = grid_mask(positions, positions, lambda r, c: r == c).astype(jnp.float32)
+    running_row = exact_dot(side, upto)
+    running_col = exact_dot(upto, side, ((0,), (1,)))
+    side_col = exact_dot(eye, side, ((1,), (1,)))
+    lower = grid_mask(positions, positions, lambda r, c: r >= c)
+    strict = grid_mask(positions, positions, lambda r, c: r > c)
+
+    parts = []
+    for s in range(sequences):
+        for b in range(sp_size):
+            line = b * side_rows + s
+            row = running_row[line : line + 1, :]
+            col = running_col[:, line : line + 1]
+            strength = side_col[:, line + 2 : line + 3]
+            final_log = row[:, positions - 1 : positions]
+            keys = kv_in[b, 0, s].astype(jnp.float32)
+            keys = keys * lax.rsqrt(jnp.sum(keys * keys, axis=-1, keepdims=True) + 1e-06)
+            within = jnp.where(lower, jnp.exp(jnp.where(lower, col - row, 0.0)), 0.0)
+            scaled = keys * strength
+            power = jnp.where(strict, -short_dot(scaled, keys, ((1,), (1,))) * within, 0.0)
+            targets = jnp.concatenate(
+                [kv_in[b, 1, s].astype(jnp.float32) * strength, scaled * jnp.exp(col)], axis=1
+            ).astype(jnp.bfloat16)
+            carried = (keys * jnp.exp(final_log - col)).T.astype(jnp.bfloat16)
+            parts.append([eye + power, power, targets, carried, jnp.exp(final_log)])
+    for part in parts:
+        part[1] = short_dot(part[1], part[1])
+    covered = 2
+    while covered < positions:
+        for part in parts:
+            if covered * 2 < positions:
+                both = short_dot(part[1], jnp.concatenate([part[0], part[1]], axis=1))
+                part[0] = part[0] + both[:, :positions]
+                part[1] = both[:, positions:]
+            else:
+                part[0] = part[0] + short_dot(part[1], part[0])
+        covered = covered * 2
+    for part in parts:
+        part[2] = short_dot(part[0], part[2])
+    states = []
+    for s in range(sequences):
+        state = None
+        for b in range(sp_size):
+            _, _, solved, carried, shrink = parts[s * sp_size + b]
+            fresh = solved[:, :value_width]
+            if state is None:
+                state = short_dot(carried, fresh)
+            else:
+                fresh = fresh - short_dot(solved[:, value_width:], state)
+                state = state * shrink + short_dot(carried, fresh)
+        states.append(state)
+
+    lanes = pl.ds(pl.multiple_of(me * key_width, key_width), key_width)
+    queries = query_ref[:, lanes].astype(jnp.float32)
+    new_keys = new_key_ref[:, lanes].astype(jnp.float32)
+    new_keys = new_keys * lax.rsqrt(jnp.sum(new_keys * new_keys, axis=-1, keepdims=True) + 1e-06)
+    meets = jnp.sum(queries * new_keys, axis=-1, keepdims=True)
+    row_out[...] = jnp.zeros_like(row_out)
+    for s in range(sequences):
+        state = states[s]
+        turned = state.T.astype(jnp.bfloat16)
+        for j in range(sp_size):
+            state_out[j, s] = turned[j * share : (j + 1) * share, :]
+        wide = (8, key_width)
+        query_read = exact_dot(jnp.broadcast_to(queries[s : s + 1], wide), state)[:1]
+        key_read = exact_dot(jnp.broadcast_to(new_keys[s : s + 1], wide), state)[:1]
+        new_value = jnp.sum(side_in[:, 4 + s, :], axis=0, keepdims=True)
+        raw = query_read + (next_strength_ref[s, me] * meets[s : s + 1]) * (new_value - key_read)
+        row_out[s : s + 1, :] = raw * lax.rsqrt(
+            jnp.sum(raw * raw, axis=-1, keepdims=True) / value_width + 1e-06
+        )
+
+    def final(n, source, sink, target, origin):
+        return pltpu.make_async_remote_copy(
+            src_ref=source,
+            dst_ref=sink.at[origin],
+            send_sem=last_send.at[n, target],
+            recv_sem=last_recv.at[n, origin],
+            device_id={"sp": target},
+            device_id_type=MESH,
+        )
+
+    for offset in range(1, sp_size):
+        target = (me + offset) % sp_size
+        final(0, state_out.at[target], state_in, target, me).start()
+        final(1, row_out, row_in, target, me).start()
+    kept = [
+        pltpu.make_async_copy(state_out.at[me], state_in.at[me], last_local.at[0]),
+        pltpu.make_async_copy(row_out, row_in.at[me], last_local.at[1]),
+    ]
+    for copy in kept:
+        copy.start()
+    for copy in kept:
+        copy.wait()
+    for offset in range(1, sp_size):
+        source = (me + offset) % sp_size
+        final(0, state_in.at[source], state_in, source, source).wait_recv()
+        final(1, row_in.at[source], row_in, source, source).wait_recv()
+
+    picker = grid_mask(value_width, share, lambda r, c: r == me * share + c).astype(jnp.float32)
+    row_lines = row_in.shape[1]
+    rows = exact_dot(row_in[...].reshape(sp_size * row_lines, value_width), picker)
+    rows = rows * gain_ref[...].reshape(1, share)
+    for s in range(sequences):
+        read_ref[s] = jnp.concatenate(
+            [rows[i * row_lines + s : i * row_lines + s + 1] for i in range(sp_size)], axis=0
+        ).astype(jnp.bfloat16)
+        for i in range(sp_size):
+            state_ref[s, i] = state_in[i, s].astype(jnp.float32).T.astype(jnp.bfloat16)
+
+    for offset in range(1, sp_size):
+        target = (me + offset) % sp_size
+        for copy in swap(target, me):
+            copy.wait_send()
+        final(0, state_out.at[target], state_in, target, me).wait_send()
+        final(1, row_out, row_in, target, me).wait_send()
+    for distance in range(chips):
+        for way, step in ((0, -1), (1, 1)):
+            if distance == 0 and way == 1:
+                continue
+            origin_chip = chip + step * distance
+            origin = origin_chip * CORES + core
+
+            @pl.when((origin_chip >= 0) & (origin_chip < chips))
+            def _(origin=origin):
+                for s in range(sequences):
+                    piece(origin, s, 2, partner).wait_send()
+
+            for other, onward in ((0, chip + 1), (1, chip - 1)):
+                if distance and other != way:
+                    continue
+
+                @pl.when(
+                    (origin_chip >= 0)
+                    & (origin_chip < chips)
+                    & (onward >= 0)
+                    & (onward < chips)
+                )
+                def _(origin=origin, other=other, onward=onward):
+                    for s in range(sequences):
+                        piece(origin, s, other, onward * CORES + core).wait_send()
+
+
+def local_fused(
+    tokens,
+    key_matrix,
+    value_matrix,
+    gate_matrix,
+    head_decay_rate,
+    extra_log_decay,
+    next_token_query,
+    next_token_key,
+    next_token_value,
+    next_write_strength,
+    read_norm_gain,
+):
+    sequences, positions, depth = tokens.shape
+    local_heads = head_decay_rate.shape[0]
+    sp_size = lax.axis_size("sp")
+    tp_size = lax.axis_size("tp")
+    key_total = key_matrix.shape[1]
+    value_total = value_matrix.shape[1]
+    key_width = key_total // local_heads
+    value_width = value_total // local_heads
+    share = value_width // sp_size
+    rows = sequences * positions
+    side_rows = 8 * ((3 * sequences + 7) // 8)
+    row_lines = 8 * ((sequences + 7) // 8)
+    vmem = pl.BlockSpec(memory_space=pltpu.VMEM)
+    smem = pl.BlockSpec(memory_space=pltpu.SMEM)
+    anywhere = pl.BlockSpec(memory_space=pl.ANY)
+    dma = pltpu.SemaphoreType.DMA
+    return pl.pallas_call(
+        functools.partial(fused_kernel, sp_size, tp_size),
+        out_shape=(
+            jax.ShapeDtypeStruct((sequences, local_heads, key_width, share), jnp.bfloat16),
+            jax.ShapeDtypeStruct((sequences, local_heads, share), jnp.bfloat16),
+        ),
+        in_specs=[smem, smem, anywhere, anywhere, anywhere] + [vmem] * 6,
+        out_specs=(vmem, vmem),
+        scratch_shapes=[
+            pltpu.VMEM((tp_size, sequences, positions, depth), jnp.bfloat16),
+            pltpu.VMEM(key_matrix.shape, jnp.bfloat16),
+            pltpu.VMEM(value_matrix.shape, jnp.bfloat16),
+            pltpu.VMEM((rows, key_total), jnp.float32),
+            pltpu.VMEM((rows, value_total), jnp.float32),
+            pltpu.VMEM((rows, gate_matrix.shape[1]), jnp.float32),
+            pltpu.VMEM((sp_size, 2, sequences, positions, key_width), jnp.bfloat16),
+            pltpu.VMEM((sp_size, 2, sequences, positions, key_width), jnp.bfloat16),
+            pltpu.VMEM((sp_size, side_rows, positions), jnp.float32),
+            pltpu.VMEM((sp_size, side_rows, positions), jnp.float32),
+            pltpu.VMEM((sp_size, sequences, share, key_width), jnp.bfloat16),
+            pltpu.VMEM((sp_size, sequences, share, key_width), jnp.bfloat16),
+            pltpu.VMEM((row_lines, value_width), jnp.float32),
+            pltpu.VMEM((sp_size, row_lines, value_width), jnp.float32),
+            dma((sequences,)),
+            dma((2,)),
+            dma((tp_size, sequences)),
+            dma((tp_size, sequences, 3)),
+            dma((2, sp_size)),
+            dma((2, sp_size)),
+            dma((2,)),
+            dma((2, sp_size)),
+            dma((2, sp_size)),
+            dma((2,)),
+        ],
+        compiler_params=pltpu.CompilerParams(
+            collective_id=0, has_side_effects=True, vmem_limit_bytes=48 * 1024 * 1024
+        ),
+    )(
+        head_decay_rate,
+        next_write_strength,
+        tokens,
+        key_matrix,
+        value_matrix,
+        gate_matrix,
+        extra_log_decay,
+        next_token_query,
+        next_token_key,
+        next_token_value,
+        read_norm_gain,
+    )
+
+
+def local(*arguments):
+    tokens, key_matrix, value_matrix = arguments[:3]
+    sequences, positions, _ = tokens.shape
+    local_heads = arguments[4].shape[0]
+    sp_size = lax.axis_size("sp")
+    fits = (
+        local_heads == sp_size
+        and sequences == 2
+        and lax.axis_size("tp") % CORES == 0
+        and positions == key_matrix.shape[1] // local_heads
+        and positions == value_matrix.shape[1] // local_heads
+        and positions % 128 == 0
+    )
+    return local_fused(*arguments) if fits else local_general(*arguments)
+
+
 def solution(mesh):
     in_specs = (
         P(None, "sp", "tp"),

time: 130 us -> 54 us (0.42)
  waiting for transfers between devices: 65 us -> 0 us
  Pallas kernels: 0 us -> 42.3 us
  matrix products: 23.3 us -> 0 us
  between operations: 14.4 us -> 0.66 us
  blocking collectives: 8.86 us -> 0 us
  starting transfers between devices: 7.41 us -> 0 us
  other arithmetic: 5.62 us -> 0 us
  local copies, waits for them, and re-layouts: 5.17 us -> 10.7 us
    pallas_call x0 -> x1, Pallas kernels: none -> 42.3 us  [local_fused(): pl.pallas_call(functools.partial(fused_kernel, sp_size, tp_size), out_sha...]
    all_to_all x2 -> x0, waiting for transfers between devices: 32.6 us -> none  [the longest x1 24.1 us: local(): lax.all_to_all(carry_copies, 'sp', split_axis=0, concat_axis=0, tiled=True)]
    all_gather x1 -> x0, waiting for transfers between devices: 31.8 us -> none  [local(): incoming = lax.all_gather(tokens, 'tp', axis=2, tiled=True)]
    dot_general x27 -> x0, matrix products: 23.3 us -> none  [the longest x1 4.21 us: local(): jnp.dot(flat_rows, key_matrix, preferred_element_type=jnp.float32)]
    unnamed x16 -> x20, local copies, waits for them, and re-layouts: 0.5 us -> 9.95 us
    psum x1 -> x0, blocking collectives: 8.86 us -> none  [local(): lax.psum(jnp.sum(read_raw * read_raw, axis=-1, keepdims=True), 'sp')]
    all_to_all x2 -> x0, starting transfers between devices: 7.37 us -> none  [the longest x1 3.74 us: local(): lax.all_to_all(carry_copies, 'sp', split_axis=0, concat_axis=0, tiled=True)]
    broadcast_in_dim x1 -> x0, local copies, waits for them, and re-layouts: 1.58 us -> none  [local(): jnp.broadcast_to(carry_map[None], (group_size,) + carry_map.shape)]
  transfers between devices with their start and end apart: 3 -> 0, of which waited for: 3 -> 0; matrix products, arithmetic and copies ran while one was open for 2% -> 0% of each run, Pallas kernels for 0% -> 0%
where the time goes in v1:
time: 54 us; the launch traced here: 53.7 us
  Pallas kernels  42.3 us (78%)
  local copies, waits for them, and re-layouts  10.7 us (20%)
  between operations  0.66 us (1%)
    pallas_call x1, Pallas kernels, local_fused(): pl.pallas_call(functools.partial(fused_kernel, sp_size, tp_size), out_sha...  42.3 us
    unnamed x20, local copies, waits for them, and re-layouts  9.95 us

profile of v1, /device:TPU:0, one launch (start us, length us, event | category | flops | bytes accessed | tf_op | source)
XLA Modules:
  0.0 53.7 jit_solution(17897605032784582370)
XLA Ops:
  0.6 1.5 %copy.13.gate_ref = bf16[4096,64]{1,0:T(8,128)(2,1)S(1)} copy(bf16[4096,64]{0,1:T(8,128)(2,1)} %param.14) | data formatting | bytes 1048576 | tf_op args[3]
  2.2 0.0 copy-start
  2.2 2.2 %copy-done = bf16[4096,512]{1,0:T(8,128)(2,1)S(1)} copy-done((bf16[4096,512]{1,0:T(8,128)(2,1)S(1)}, bf16[4096,512]{1,0:T(8,128)(2,1)}, u32[]{:S(2)}) %copy-start) | copy-done | bytes 4194328
  4.3 0.0 copy-start.1
  4.3 0.9 %copy-done.1 = bf16[2,128,512]{2,1,0:T(8,128)(2,1)S(1)} copy-done((bf16[2,128,512]{2,1,0:T(8,128)(2,1)S(1)}, bf16[2,128,512]{2,1,0:T(8,128)(2,1)}, u32[]{:S(2)}) %copy-start.1) | copy-done | bytes 262168
  5.3 0.0 copy-start.2
  5.3 0.7 %copy-done.2 = f32[2,4,128]{2,1,0:T(4,128)S(1)} copy-done((f32[2,4,128]{2,1,0:T(4,128)S(1)}, f32[2,4,128]{2,1,0:T(4,128)}, u32[]{:S(2)}) %copy-start.2) | copy-done | bytes 4120
  6.0 0.0 copy-start.3
  6.0 0.7 %copy-done.3 = bf16[2,512]{1,0:T(2,128)(2,1)S(1)} copy-done((bf16[2,512]{1,0:T(2,128)(2,1)S(1)}, bf16[2,512]{1,0:T(2,128)(2,1)}, u32[]{:S(2)}) %copy-start.3) | copy-done | bytes 2072
  6.7 0.0 copy-start.4
  6.7 0.7 %copy-done.4 = bf16[2,512]{1,0:T(2,128)(2,1)S(1)} copy-done((bf16[2,512]{1,0:T(2,128)(2,1)S(1)}, bf16[2,512]{1,0:T(2,128)(2,1)}, u32[]{:S(2)}) %copy-start.4) | copy-done | bytes 2072
  7.3 0.0 copy-start.5
  7.3 0.7 %copy-done.5 = bf16[2,4,32]{2,1,0:T(4,128)(2,1)S(1)} copy-done((bf16[2,4,32]{2,1,0:T(4,128)(2,1)S(1)}, bf16[2,4,32]{2,1,0:T(4,128)(2,1)}, u32[]{:S(2)}) %copy-start.5) | copy-done | bytes 536
  8.0 0.0 copy-start.6
  8.0 0.7 %copy-done.6 = f32[2,4]{1,0:T(2,128)S(1)} copy-done((f32[2,4]{1,0:T(2,128)S(1)}, f32[2,4]{1,0:T(2,128)}, u32[]{:S(2)}) %copy-start.6) | copy-done | bytes 56
  8.7 0.0 copy-start.7
  8.7 0.7 %copy-done.7 = f32[4]{0:T(128)S(1)} copy-done((f32[4]{0:T(128)S(1)}, f32[4]{0:T(128)}, u32[]{:S(2)}) %copy-start.7) | copy-done | bytes 40
  9.4 0.0 copy-start.8
  9.4 0.7 %copy-done.8 = f32[32]{0:T(128)S(1)} copy-done((f32[32]{0:T(128)S(1)}, f32[32]{0:T(128)}, u32[]{:S(2)}) %copy-start.8) | copy-done | bytes 152
  10.0 42.3 %shard_map.122 = (bf16[2,4,128,32]{3,2,1,0:T(8,128)(2,1)S(1)}, bf16[2,4,32]{2,1,0:T(4,128)(2,1)S(1)}) custom-call(f32[4]{0:T(128)S(1)} %copy-done.7, f32[2,4]{1,0:T(2,128)S(1)} %copy-done.6, bf16[2,128,512]{2,1,0:T(8,128)(2,1)S(1)} %copy-done.1, bf16[4096,512]{1,0:T(8,128)(2,1)S(1)} %copy-done, bf16[4096,512]{1,0:T(8,128)(2,1)} %value_ref.1, ...), custom_call_target="tpu_custom_call" | custom-call | tf_op jit(solution)/shard_map/pallas_call | solution.py:612
  52.3 0.8 %copy.14 = bf16[2,4,128,32]{2,3,1,0:T(8,128)(2,1)} copy(bf16[2,4,128,32]{3,2,1,0:T(8,128)(2,1)S(1)} %get-tuple-element.2) | data formatting | bytes 131072 | tf_op jit(solution)/shard_map/pallas_call | solution.py:612
  53.1 0.6 %copy.16 = bf16[2,4,32]{2,1,0:T(4,128)(2,1)} copy(bf16[2,4,32]{2,1,0:T(4,128)(2,1)S(1)} %get-tuple-element.7) | data formatting | bytes 1024
Async XLA Ops:
  2.2 2.2 %copy-start = (bf16[4096,512]{1,0:T(8,128)(2,1)S(1)}, bf16[4096,512]{1,0:T(8,128)(2,1)}, u32[]{:S(2)}) copy-start(bf16[4096,512]{1,0:T(8,128)(2,1)} %key_ref.1) | copy-start | bytes 12582916
  4.3 0.9 %copy-start.1 = (bf16[2,128,512]{2,1,0:T(8,128)(2,1)S(1)}, bf16[2,128,512]{2,1,0:T(8,128)(2,1)}, u32[]{:S(2)}) copy-start(bf16[2,128,512]{2,1,0:T(8,128)(2,1)} %tokens_ref.1) | copy-start | bytes 786436
  5.3 0.7 %copy-start.2 = (f32[2,4,128]{2,1,0:T(4,128)S(1)}, f32[2,4,128]{2,1,0:T(4,128)}, u32[]{:S(2)}) copy-start(f32[2,4,128]{2,1,0:T(4,128)} %extra_ref.1) | copy-start | bytes 12292
  6.0 0.7 %copy-start.3 = (bf16[2,512]{1,0:T(2,128)(2,1)S(1)}, bf16[2,512]{1,0:T(2,128)(2,1)}, u32[]{:S(2)}) copy-start(bf16[2,512]{1,0:T(2,128)(2,1)} %query_ref.1) | copy-start | bytes 6148
  6.7 0.7 %copy-start.4 = (bf16[2,512]{1,0:T(2,128)(2,1)S(1)}, bf16[2,512]{1,0:T(2,128)(2,1)}, u32[]{:S(2)}) copy-start(bf16[2,512]{1,0:T(2,128)(2,1)} %new_key_ref.1) | copy-start | bytes 6148
  7.3 0.7 %copy-start.5 = (bf16[2,4,32]{2,1,0:T(4,128)(2,1)S(1)}, bf16[2,4,32]{2,1,0:T(4,128)(2,1)}, u32[]{:S(2)}) copy-start(bf16[2,4,32]{2,1,0:T(4,128)(2,1)} %new_value_ref.1) | copy-start | bytes 1540
  8.0 0.7 %copy-start.6 = (f32[2,4]{1,0:T(2,128)S(1)}, f32[2,4]{1,0:T(2,128)}, u32[]{:S(2)}) copy-start(f32[2,4]{1,0:T(2,128)} %next_strength_ref.1) | copy-start | bytes 100
  8.7 0.7 %copy-start.7 = (f32[4]{0:T(128)S(1)}, f32[4]{0:T(128)}, u32[]{:S(2)}) copy-start(f32[4]{0:T(128)} %rate_ref.1) | copy-start | bytes 52
  9.4 0.7 %copy-start.8 = (f32[32]{0:T(128)S(1)}, f32[32]{0:T(128)}, u32[]{:S(2)}) copy-start(f32[32]{0:T(128)} %gain_ref.1) | copy-start | bytes 388

commit v2 on v1

--- a/solution.py
+++ b/solution.py
@@ -216,17 +216,23 @@
     tokens_ref,
     key_ref,
     value_ref,
+    gate_hbm,
+    extra_hbm,
+    query_hbm,
+    new_key_hbm,
+    new_value_hbm,
+    gain_hbm,
+    state_ref,
+    read_ref,
+    gathered,
+    key_w,
+    value_w,
     gate_ref,
     extra_ref,
     query_ref,
     new_key_ref,
     new_value_ref,
     gain_ref,
-    state_ref,
-    read_ref,
-    gathered,
-    key_w,
-    value_w,
     key_acc,
     value_acc,
     gate_acc,
@@ -254,7 +260,7 @@
     key_width = key_acc.shape[1] // local_heads
     value_width = value_acc.shape[1] // local_heads
     share = value_width // sp_size
-    all_heads = gate_ref.shape[1] // 2
+    all_heads = gate_ref.shape[0] // 2
     chips = tp_size // CORES
     me = lax.axis_index("sp")
     spot = lax.axis_index("tp")
@@ -287,12 +293,20 @@
     weights = [
         pltpu.make_async_copy(key_ref, key_w, weight_sem.at[0]),
         pltpu.make_async_copy(value_ref, value_w, weight_sem.at[1]),
+        pltpu.make_async_copy(gate_hbm, gate_ref, weight_sem.at[2]),
+        pltpu.make_async_copy(extra_hbm, extra_ref, weight_sem.at[3]),
+        pltpu.make_async_copy(query_hbm, query_ref, weight_sem.at[4]),
+        pltpu.make_async_copy(new_key_hbm, new_key_ref, weight_sem.at[5]),
+        pltpu.make_async_copy(new_value_hbm, new_value_ref, weight_sem.at[6]),
+        pltpu.make_async_copy(gain_hbm, gain_ref, weight_sem.at[7]),
     ]
     for weight in weights:
         weight.start()
     key_acc[...] = jnp.zeros_like(key_acc)
     value_acc[...] = jnp.zeros_like(value_acc)
     gate_acc[...] = jnp.zeros_like(gate_acc)
+    side_out[...] = jnp.zeros_like(side_out)
+    row_out[...] = jnp.zeros_like(row_out)
     for load in loads:
         load.wait()
     near = jnp.where(chip > 0, 1, 0) + jnp.where(chip < chips - 1, 1, 0)
@@ -308,12 +322,68 @@
             device_id_type=MESH,
         )
 
-    def take(block):
-        rows = gathered[block].reshape(sequences * positions, depth)
+    def take(block, s):
+        rows = gathered[block, s]
+        cut = slice(s * positions, (s + 1) * positions)
         span = pl.ds(pl.multiple_of(block * depth, depth), depth)
-        key_acc[...] += jnp.dot(rows, key_w[span, :], preferred_element_type=jnp.float32)
-        value_acc[...] += jnp.dot(rows, value_w[span, :], preferred_element_type=jnp.float32)
-        gate_acc[...] += jnp.dot(rows, gate_ref[span, :], preferred_element_type=jnp.float32)
+        key_acc[cut] += jnp.dot(rows, key_w[span, :], preferred_element_type=jnp.float32)
+        value_acc[cut] += jnp.dot(rows, value_w[span, :], preferred_element_type=jnp.float32)
+        gate_acc[cut] += lax.dot_general(
+            rows,
+            gate_ref[:, span],
+            (((1,), (1,)), ((), ())),
+            preferred_element_type=jnp.float32,
+        )
+
+    first = spot * local_heads
+    chooser = grid_mask(
+        2 * local_heads,
+        2 * all_heads,
+        lambda r, c: c == jnp.where(r < local_heads, first + r, all_heads + first + r - local_heads),
+    ).astype(jnp.float32)
+    placer = grid_mask(share, value_width, lambda r, c: c == me * share + r).astype(jnp.float32)
+
+    def swap(s, target, origin):
+        return [
+            pltpu.make_async_remote_copy(
+                src_ref=source.at[target, s],
+                dst_ref=sink.at[origin, s],
+                send_sem=swap_send.at[n, s, target],
+                recv_sem=swap_recv.at[n, s, origin],
+                device_id={"sp": target},
+                device_id_type=MESH,
+            )
+            for n, (source, sink) in enumerate(((kv_out, kv_in), (side_out, side_in)))
+        ]
+
+    def kept(s):
+        return [
+            pltpu.make_async_copy(kv_out.at[me, s], kv_in.at[me, s], swap_local.at[0, s]),
+            pltpu.make_async_copy(side_out.at[me, s], side_in.at[me, s], swap_local.at[1, s]),
+        ]
+
+    def hand_out(s):
+        cut = slice(s * positions, (s + 1) * positions)
+        gates = exact_dot(chooser, gate_acc[cut], ((1,), (1,)))
+        new_value = exact_dot(new_value_ref[s].astype(jnp.float32), placer)
+        extra = extra_ref[s]
+        for h in range(local_heads):
+            kv_out[h, s, 0] = key_acc[cut, h * key_width : (h + 1) * key_width].astype(jnp.bfloat16)
+            kv_out[h, s, 1] = value_acc[cut, h * value_width : (h + 1) * value_width].astype(
+                jnp.bfloat16
+            )
+            side_out[h, s, 0:1, :] = (
+                -rate_ref[h] * softplus(gates[h : h + 1]) + extra[h : h + 1, :]
+            )
+            side_out[h, s, 1:2, :] = jax.nn.sigmoid(
+                gates[local_heads + h : local_heads + h + 1] - strength_offset
+            )
+            side_out[h, s, 2:3, :] = new_value[h : h + 1, :]
+        for offset in range(1, sp_size):
+            for copy in swap(s, (me + offset) % sp_size, me):
+                copy.start()
+        for copy in kept(s):
+            copy.start()
 
     for s in range(sequences):
 
@@ -328,10 +398,10 @@
         piece(spot, s, 2, partner).start()
     for weight in weights:
         weight.wait()
-    take(spot)
     for s in range(sequences):
+        take(spot, s)
         piece(partner, s, 2, partner).wait_recv()
-    take(partner)
+        take(partner, s)
 
     for distance in range(1, chips):
         for s in range(sequences):
@@ -351,208 +421,150 @@
 
                     piece(origin, s, 2, partner).start()
 
-        def absorb(index, carry, distance=distance):
-            side = index // CORES
-            which = index % CORES
-            origin_chip = chip + (2 * side - 1) * distance
-            present = (origin_chip >= 0) & (origin_chip < chips)
-
-            @pl.when(present & (which == 0))
-            def _():
-                take(origin_chip * CORES + core)
-
-            @pl.when(present & (which == 1))
-            def _():
-                block = origin_chip * CORES + 1 - core
-                for s in range(sequences):
+            def absorb(index, carry, distance=distance, s=s):
+                side = index // CORES
+                which = index % CORES
+                origin_chip = chip + (2 * side - 1) * distance
+                present = (origin_chip >= 0) & (origin_chip < chips)
+
+                @pl.when(present & (which == 0))
+                def _():
+                    take(origin_chip * CORES + core, s)
+
+                @pl.when(present & (which == 1))
+                def _():
+                    block = origin_chip * CORES + 1 - core
                     piece(block, s, 2, partner).wait_recv()
-                take(block)
-
-            return carry
-
-        lax.fori_loop(0, 2 * CORES, absorb, 0)
-
-    first = spot * local_heads
-    chooser = grid_mask(
-        2 * local_heads,
-        2 * all_heads,
-        lambda r, c: c == jnp.where(r < local_heads, first + r, all_heads + first + r - local_heads),
-    ).astype(jnp.float32)
-    gates = exact_dot(chooser, gate_acc[...], ((1,), (1,)))
-    placer = grid_mask(share, value_width, lambda r, c: c == me * share + r).astype(jnp.float32)
-    side_out[...] = jnp.zeros_like(side_out)
-    for s in range(sequences):
-        cut = slice(s * positions, (s + 1) * positions)
-        new_value = exact_dot(new_value_ref[s].astype(jnp.float32), placer)
-        extra = extra_ref[s]
-        for h in range(local_heads):
-            kv_out[h, 0, s] = key_acc[cut, h * key_width : (h + 1) * key_width].astype(jnp.bfloat16)
-            kv_out[h, 1, s] = value_acc[cut, h * value_width : (h + 1) * value_width].astype(
-                jnp.bfloat16
-            )
-            side_out[h, s : s + 1, :] = (
-                -rate_ref[h] * softplus(gates[h : h + 1, cut]) + extra[h : h + 1, :]
-            )
-            side_out[h, 2 + s : 3 + s, :] = jax.nn.sigmoid(
-                gates[local_heads + h : local_heads + h + 1, cut] - strength_offset
-            )
-            side_out[h, 4 + s : 5 + s, :] = new_value[h : h + 1, :]
-
-    def swap(target, origin):
-        return [
-            pltpu.make_async_remote_copy(
-                src_ref=source.at[target],
-                dst_ref=sink.at[origin],
-                send_sem=swap_send.at[n, target],
-                recv_sem=swap_recv.at[n, origin],
-                device_id={"sp": target},
-                device_id_type=MESH,
-            )
-            for n, (source, sink) in enumerate(((kv_out, kv_in), (side_out, side_in)))
-        ]
-
-    for offset in range(1, sp_size):
-        for copy in swap((me + offset) % sp_size, me):
-            copy.start()
-    kept = [
-        pltpu.make_async_copy(kv_out.at[me], kv_in.at[me], swap_local.at[0]),
-        pltpu.make_async_copy(side_out.at[me], side_in.at[me], swap_local.at[1]),
-    ]
-    for copy in kept:
-        copy.start()
-    for copy in kept:
-        copy.wait()
-    for offset in range(1, sp_size):
-        source = (me + offset) % sp_size
-        for n, sink in enumerate((kv_in, side_in)):
-            pltpu.make_async_remote_copy(
-                src_ref=sink.at[source],
-                dst_ref=sink.at[source],
-                send_sem=swap_send.at[n, source],
-                recv_sem=swap_recv.at[n, source],
-                device_id={"sp": source},
-                device_id_type=MESH,
-            ).wait_recv()
-
-    side_rows = side_in.shape[1]
-    side = side_in[...].reshape(sp_size * side_rows, positions)
+                    take(block, s)
+
+                return carry
+
+            lax.fori_loop(0, 2 * CORES, absorb, 0)
+            if distance == chips - 1:
+                hand_out(s)
+
+    side_rows = side_in.shape[2]
     upto = grid_mask(positions, positions, lambda r, c: r <= c).astype(jnp.float32)
     eye = grid_mask(positions, positions, lambda r, c: r == c).astype(jnp.float32)
-    running_row = exact_dot(side, upto)
-    running_col = exact_dot(upto, side, ((0,), (1,)))
-    side_col = exact_dot(eye, side, ((1,), (1,)))
     lower = grid_mask(positions, positions, lambda r, c: r >= c)
     strict = grid_mask(positions, positions, lambda r, c: r > c)
-
-    parts = []
+    lanes = pl.ds(pl.multiple_of(me * key_width, key_width), key_width)
+    queries = query_ref[:, lanes].astype(jnp.float32)
+    new_keys = new_key_ref[:, lanes].astype(jnp.float32)
+    new_keys = new_keys * lax.rsqrt(jnp.sum(new_keys * new_keys, axis=-1, keepdims=True) + 1e-06)
+    meets = jnp.sum(queries * new_keys, axis=-1, keepdims=True)
+
+    def final(n, s, source, sink, target, origin):
+        return pltpu.make_async_remote_copy(
+            src_ref=source,
+            dst_ref=sink.at[origin, s],
+            send_sem=last_send.at[n, s, target],
+            recv_sem=last_recv.at[n, s, origin],
+            device_id={"sp": target},
+            device_id_type=MESH,
+        )
+
+    def stay(s):
+        return [
+            pltpu.make_async_copy(state_out.at[me, s], state_in.at[me, s], last_local.at[0, s]),
+            pltpu.make_async_copy(row_out.at[s], row_in.at[me, s], last_local.at[1, s]),
+        ]
+
     for s in range(sequences):
+        for copy in kept(s):
+            copy.wait()
+        for offset in range(1, sp_size):
+            source = (me + offset) % sp_size
+            for copy in swap(s, source, source):
+                copy.wait_recv()
+        side = side_in[:, s].reshape(sp_size * side_rows, positions)
+        running_row = exact_dot(side, upto)
+        running_col = exact_dot(upto, side, ((0,), (1,)))
+        side_col = exact_dot(eye, side, ((1,), (1,)))
+        parts = []
         for b in range(sp_size):
-            line = b * side_rows + s
+            line = b * side_rows
             row = running_row[line : line + 1, :]
             col = running_col[:, line : line + 1]
-            strength = side_col[:, line + 2 : line + 3]
+            strength = side_col[:, line + 1 : line + 2]
             final_log = row[:, positions - 1 : positions]
-            keys = kv_in[b, 0, s].astype(jnp.float32)
+            keys = kv_in[b, s, 0].astype(jnp.float32)
             keys = keys * lax.rsqrt(jnp.sum(keys * keys, axis=-1, keepdims=True) + 1e-06)
             within = jnp.where(lower, jnp.exp(jnp.where(lower, col - row, 0.0)), 0.0)
             scaled = keys * strength
             power = jnp.where(strict, -short_dot(scaled, keys, ((1,), (1,))) * within, 0.0)
             targets = jnp.concatenate(
-                [kv_in[b, 1, s].astype(jnp.float32) * strength, scaled * jnp.exp(col)], axis=1
+                [kv_in[b, s, 1].astype(jnp.float32) * strength, scaled * jnp.exp(col)], axis=1
             ).astype(jnp.bfloat16)
             carried = (keys * jnp.exp(final_log - col)).T.astype(jnp.bfloat16)
             parts.append([eye + power, power, targets, carried, jnp.exp(final_log)])
-    for part in parts:
-        part[1] = short_dot(part[1], part[1])
-    covered = 2
-    while covered < positions:
         for part in parts:
-            if covered * 2 < positions:
-                both = short_dot(part[1], jnp.concatenate([part[0], part[1]], axis=1))
-                part[0] = part[0] + both[:, :positions]
-                part[1] = both[:, positions:]
-            else:
-                part[0] = part[0] + short_dot(part[1], part[0])
-        covered = covered * 2
-    for part in parts:
-        part[2] = short_dot(part[0], part[2])
-    states = []
-    for s in range(sequences):
+            part[1] = short_dot(part[1], part[1])
+        covered = 2
+        while covered < positions:
+            for part in parts:
+                if covered * 2 < positions:
+                    both = short_dot(part[1], jnp.concatenate([part[0], part[1]], axis=1))
+                    part[0] = part[0] + both[:, :positions]
+                    part[1] = both[:, positions:]
+                else:
+                    part[0] = part[0] + short_dot(part[1], part[0])
+            covered = covered * 2
+        for part in parts:
+            part[2] = short_dot(part[0], part[2])
         state = None
-        for b in range(sp_size):
-            _, _, solved, carried, shrink = parts[s * sp_size + b]
+        for _, _, solved, carried, shrink in parts:
             fresh = solved[:, :value_width]
             if state is None:
                 state = short_dot(carried, fresh)
             else:
                 fresh = fresh - short_dot(solved[:, value_width:], state)
                 state = state * shrink + short_dot(carried, fresh)
-        states.append(state)
-
-    lanes = pl.ds(pl.multiple_of(me * key_width, key_width), key_width)
-    queries = query_ref[:, lanes].astype(jnp.float32)
-    new_keys = new_key_ref[:, lanes].astype(jnp.float32)
-    new_keys = new_keys * lax.rsqrt(jnp.sum(new_keys * new_keys, axis=-1, keepdims=True) + 1e-06)
-    meets = jnp.sum(queries * new_keys, axis=-1, keepdims=True)
-    row_out[...] = jnp.zeros_like(row_out)
-    for s in range(sequences):
-        state = states[s]
+
         turned = state.T.astype(jnp.bfloat16)
         for j in range(sp_size):
             state_out[j, s] = turned[j * share : (j + 1) * share, :]
+        for offset in range(1, sp_size):
+            target = (me + offset) % sp_size
+            final(0, s, state_out.at[target, s], state_in, target, me).start()
         wide = (8, key_width)
         query_read = exact_dot(jnp.broadcast_to(queries[s : s + 1], wide), state)[:1]
         key_read = exact_dot(jnp.broadcast_to(new_keys[s : s + 1], wide), state)[:1]
-        new_value = jnp.sum(side_in[:, 4 + s, :], axis=0, keepdims=True)
+        new_value = jnp.sum(side_in[:, s, 2, :], axis=0, keepdims=True)
         raw = query_read + (next_strength_ref[s, me] * meets[s : s + 1]) * (new_value - key_read)
-        row_out[s : s + 1, :] = raw * lax.rsqrt(
+        row_out[s, 0:1, :] = raw * lax.rsqrt(
             jnp.sum(raw * raw, axis=-1, keepdims=True) / value_width + 1e-06
         )
-
-    def final(n, source, sink, target, origin):
-        return pltpu.make_async_remote_copy(
-            src_ref=source,
-            dst_ref=sink.at[origin],
-            send_sem=last_send.at[n, target],
-            recv_sem=last_recv.at[n, origin],
-            device_id={"sp": target},
-            device_id_type=MESH,
-        )
-
-    for offset in range(1, sp_size):
-        target = (me + offset) % sp_size
-        final(0, state_out.at[target], state_in, target, me).start()
-        final(1, row_out, row_in, target, me).start()
-    kept = [
-        pltpu.make_async_copy(state_out.at[me], state_in.at[me], last_local.at[0]),
-        pltpu.make_async_copy(row_out, row_in.at[me], last_local.at[1]),
-    ]
-    for copy in kept:
-        copy.start()
-    for copy in kept:
-        copy.wait()
-    for offset in range(1, sp_size):
-        source = (me + offset) % sp_size
-        final(0, state_in.at[source], state_in, source, source).wait_recv()
-        final(1, row_in.at[source], row_in, source, source).wait_recv()
+        for offset in range(1, sp_size):
+            target = (me + offset) % sp_size
+            final(1, s, row_out.at[s], row_in, target, me).start()
+        for copy in stay(s):
+            copy.start()
 
     picker = grid_mask(value_width, share, lambda r, c: r == me * share + c).astype(jnp.float32)
-    row_lines = row_in.shape[1]
-    rows = exact_dot(row_in[...].reshape(sp_size * row_lines, value_width), picker)
-    rows = rows * gain_ref[...].reshape(1, share)
+    row_lines = row_in.shape[2]
     for s in range(sequences):
+        for copy in stay(s):
+            copy.wait()
+        for offset in range(1, sp_size):
+            source = (me + offset) % sp_size
+            final(0, s, state_in.at[source, s], state_in, source, source).wait_recv()
+            final(1, s, row_in.at[source, s], row_in, source, source).wait_recv()
+        rows = exact_dot(row_in[:, s].reshape(sp_size * row_lines, value_width), picker)
+        rows = rows * gain_ref[...].reshape(1, share)
         read_ref[s] = jnp.concatenate(
-            [rows[i * row_lines + s : i * row_lines + s + 1] for i in range(sp_size)], axis=0
+            [rows[i * row_lines : i * row_lines + 1] for i in range(sp_size)], axis=0
         ).astype(jnp.bfloat16)
         for i in range(sp_size):
-            state_ref[s, i] = state_in[i, s].astype(jnp.float32).T.astype(jnp.bfloat16)
-
-    for offset in range(1, sp_size):
-        target = (me + offset) % sp_size
-        for copy in swap(target, me):
-            copy.wait_send()
-        final(0, state_out.at[target], state_in, target, me).wait_send()
-        final(1, row_out, row_in, target, me).wait_send()
+            state_ref[s, i] = state_in[i, s]
+
+    for s in range(sequences):
+        for offset in range(1, sp_size):
+            target = (me + offset) % sp_size
+            for copy in swap(s, target, me):
+                copy.wait_send()
+            final(0, s, state_out.at[target, s], state_in, target, me).wait_send()
+            final(1, s, row_out.at[s], row_in, target, me).wait_send()
     for distance in range(chips):
         for way, step in ((0, -1), (1, 1)):
             if distance == 0 and way == 1:
@@ -603,48 +615,52 @@
     value_width = value_total // local_heads
     share = value_width // sp_size
     rows = sequences * positions
-    side_rows = 8 * ((3 * sequences + 7) // 8)
-    row_lines = 8 * ((sequences + 7) // 8)
     vmem = pl.BlockSpec(memory_space=pltpu.VMEM)
     smem = pl.BlockSpec(memory_space=pltpu.SMEM)
     anywhere = pl.BlockSpec(memory_space=pl.ANY)
     dma = pltpu.SemaphoreType.DMA
-    return pl.pallas_call(
+    turned, read = pl.pallas_call(
         functools.partial(fused_kernel, sp_size, tp_size),
         out_shape=(
-            jax.ShapeDtypeStruct((sequences, local_heads, key_width, share), jnp.bfloat16),
+            jax.ShapeDtypeStruct((sequences, local_heads, share, key_width), jnp.bfloat16),
             jax.ShapeDtypeStruct((sequences, local_heads, share), jnp.bfloat16),
         ),
-        in_specs=[smem, smem, anywhere, anywhere, anywhere] + [vmem] * 6,
+        in_specs=[smem, smem] + [anywhere] * 9,
         out_specs=(vmem, vmem),
         scratch_shapes=[
             pltpu.VMEM((tp_size, sequences, positions, depth), jnp.bfloat16),
             pltpu.VMEM(key_matrix.shape, jnp.bfloat16),
             pltpu.VMEM(value_matrix.shape, jnp.bfloat16),
+            pltpu.VMEM(gate_matrix.shape[::-1], jnp.bfloat16),
+            pltpu.VMEM(extra_log_decay.shape, jnp.float32),
+            pltpu.VMEM(next_token_query.shape, jnp.bfloat16),
+            pltpu.VMEM(next_token_key.shape, jnp.bfloat16),
+            pltpu.VMEM(next_token_value.shape, jnp.bfloat16),
+            pltpu.VMEM(read_norm_gain.shape, jnp.float32),
             pltpu.VMEM((rows, key_total), jnp.float32),
             pltpu.VMEM((rows, value_total), jnp.float32),
             pltpu.VMEM((rows, gate_matrix.shape[1]), jnp.float32),
-            pltpu.VMEM((sp_size, 2, sequences, positions, key_width), jnp.bfloat16),
-            pltpu.VMEM((sp_size, 2, sequences, positions, key_width), jnp.bfloat16),
-            pltpu.VMEM((sp_size, side_rows, positions), jnp.float32),
-            pltpu.VMEM((sp_size, side_rows, positions), jnp.float32),
+            pltpu.VMEM((sp_size, sequences, 2, positions, key_width), jnp.bfloat16),
+            pltpu.VMEM((sp_size, sequences, 2, positions, key_width), jnp.bfloat16),
+            pltpu.VMEM((sp_size, sequences, 8, positions), jnp.float32),
+            pltpu.VMEM((sp_size, sequences, 8, positions), jnp.float32),
             pltpu.VMEM((sp_size, sequences, share, key_width), jnp.bfloat16),
             pltpu.VMEM((sp_size, sequences, share, key_width), jnp.bfloat16),
-            pltpu.VMEM((row_lines, value_width), jnp.float32),
-            pltpu.VMEM((sp_size, row_lines, value_width), jnp.float32),
+            pltpu.VMEM((sequences, 8, value_width), jnp.float32),
+            pltpu.VMEM((sp_size, sequences, 8, value_width), jnp.float32),
             dma((sequences,)),
-            dma((2,)),
+            dma((8,)),
             dma((tp_size, sequences)),
             dma((tp_size, sequences, 3)),
-            dma((2, sp_size)),
-            dma((2, sp_size)),
-            dma((2,)),
-            dma((2, sp_size)),
-            dma((2, sp_size)),
-            dma((2,)),
+            dma((2, sequences, sp_size)),
+            dma((2, sequences, sp_size)),
+            dma((2, sequences)),
+            dma((2, sequences, sp_size)),
+            dma((2, sequences, sp_size)),
+            dma((2, sequences)),
         ],
         compiler_params=pltpu.CompilerParams(
-            collective_id=0, has_side_effects=True, vmem_limit_bytes=48 * 1024 * 1024
+            collective_id=0, has_side_effects=True
         ),
     )(
         head_decay_rate,
@@ -652,13 +668,14 @@
         tokens,
         key_matrix,
         value_matrix,
-        gate_matrix,
+        gate_matrix.T,
         extra_log_decay,
         next_token_query,
         next_token_key,
         next_token_value,
         read_norm_gain,
     )
+    return jnp.swapaxes(turned, 2, 3), read
 
 
 def local(*arguments):
@@ -670,6 +687,7 @@
         local_heads == sp_size
         and sequences == 2
         and lax.axis_size("tp") % CORES == 0
+        and lax.axis_size("tp") > CORES
         and positions == key_matrix.shape[1] // local_heads
         and positions == value_matrix.shape[1] // local_heads
         and positions % 128 == 0

time: 54 us -> 43.1 us (0.80)
  local copies, waits for them, and re-layouts: 10.7 us -> 2.72 us
  Pallas kernels: 42.3 us -> 39.6 us
    unnamed x20 -> x2, local copies, waits for them, and re-layouts: 9.95 us -> 2.72 us
    pallas_call x1, Pallas kernels: 42.3 us -> 39.6 us  [local_fused(): pl.pallas_call(functools.partial(fused_kernel, sp_size, tp_size), out_sha...]
    pallas_call x1 -> x0, local copies, waits for them, and re-layouts: 0.75 us -> none  [local_fused(): pl.pallas_call(functools.partial(fused_kernel, sp_size, tp_size), out_sha...]
where the time goes in v2:
time: 43.1 us; the launch traced here: 42.9 us
  Pallas kernels  39.6 us (92%)
  local copies, waits for them, and re-layouts  2.72 us (6%)
  between operations  0.64 us (1%)
    pallas_call x1, Pallas kernels, local_fused(): pl.pallas_call(functools.partial(fused_kernel, sp_size, tp_size), out_sha...  39.6 us
    unnamed x2, local copies, waits for them, and re-layouts  2.72 us

profile of v2, /device:TPU:0, one launch (start us, length us, event | category | flops | bytes accessed | tf_op | source)
XLA Modules:
  0.0 42.9 jit_solution(16981895077150305438)
XLA Ops:
  0.6 39.6 %shard_map.122 = (bf16[2,4,32,128]{3,2,1,0:T(8,128)(2,1)}, bf16[2,4,32]{2,1,0:T(4,128)(2,1)}) custom-call(f32[4]{0:T(128)} %rate_ref.1, f32[2,4]{1,0:T(2,128)} %next_strength_ref.1, bf16[2,128,512]{2,1,0:T(8,128)(2,1)} %tokens_ref.1, bf16[4096,512]{1,0:T(8,128)(2,1)} %key_ref.1, bf16[4096,512]{1,0:T(8,128)(2,1)} %value_ref.1, bf16[64,4096]{1,0:T(8,128)(2,1)} %bitcast.2, ...), custom_call_target="tpu_custom_call" | custom-call | tf_op jit(solution)/shard_map/pallas_call | solution.py:622
  40.2 1.5 %copy.15 = bf16[2,4,128,32]{2,3,1,0:T(8,128)(2,1)} copy(bf16[2,4,128,32]{2,3,1,0:T(8,128)(2,1)} %bitcast.3) | data formatting | bytes 131072
  41.7 1.2 %copy.16 = bf16[2,4,32]{2,1,0:T(4,128)(2,1)} copy(bf16[2,4,32]{2,1,0:T(4,128)(2,1)} %get-tuple-element.9) | data formatting | bytes 1024
